TPU v7x, 32 devices: a whole 2x2x4 slice. The times are simulated.
32 devices in a mesh: sp: 4 (over x, core), tp: 8 (over z, y).
Axes of the slice: x: 2, y: 2, z: 4, core: 2. Of those that a mesh axis runs over, the one named last changes fastest.
Arguments:
- tokens: bfloat16 [4, 1024, 2048], P(None, ('sp', 'tp')), may hold values from -6 to 6
- norm_gain: float32 [2048], replicated, may hold values from 0.5 to 1.5
- entry_projection: bfloat16 [2048, 2048], P(None, 'tp'), may hold values from -0.125 to 0.125
- valve_projection: bfloat16 [2048, 2048], P(None, 'tp'), may hold values from -0.125 to 0.125
- filter_taps: float32 [4, 2048], P(None, 'tp'), may hold values from -3 to 3
- conv_bias: float32 [2048], P('tp'), may hold values from -0.6 to 0.6
- recur_weight: bfloat16 [16, 128, 128], P('tp'), may hold values from -0.5 to 0.5
- recur_bias: float32 [2048], P('tp'), may hold values from -3 to 3
- entry_weight: bfloat16 [16, 128, 128], P('tp'), may hold values from -0.5 to 0.5
- entry_bias: float32 [2048], P('tp'), may hold values from -0.6 to 0.6
- forget_rate: float32 [2048], P('tp'), may hold values from 6.1035156e-05 to 0.25, as said below
- output_weight: bfloat16 [2048, 2048], P('tp'), may hold values from -0.5 to 0.5
Outputs:
- mixed: bfloat16 [4, 1024, 2048], P(None, ('sp', 'tp'))
Inputs may be any that keep to these rules, and one draw needn't show every extreme that they name: forget_rate is positive; its even channels lie between 1 / 16384 and 1 / 4096, its odd channels between 1 / 64 and 1 / 4.
All inputs are finite; a program needn't handle non-finite values.
Results may differ from a plain program's by a relative error of at most 0.02.
Values may be sent and summed in bfloat16 or wider, within the bound.
A program may use at most 64 MiB of HBM per device.

v0:
```python
import jax
import jax.numpy as jnp
from jax import lax
from jax.sharding import PartitionSpec as P

epsilon = 1e-06
gate_power = 8.0


def over_all(shard, axis, dim, work):
    return work(lax.all_gather(shard, axis, axis=dim, tiled=True), jnp.int32(0))


def from_behind(value, axis, by):
    devices = lax.axis_size(axis)
    pairs = [(i, i + by) for i in range(devices) if 0 <= i + by < devices]
    return lax.ppermute(value, axis, pairs)


def entering_2(part, axis, combine, identity, reverse):
    count = lax.axis_size(axis)
    place = lax.axis_index(axis)
    ahead = count - 1 - place if reverse else place
    gathered = jax.tree.map(lambda a: lax.all_gather(a, axis), part)
    state = jax.tree.map(lambda a, e: jnp.zeros_like(a) + jnp.asarray(e, a.dtype), part, identity)

    def one(hop, state):
        source = count - 1 - hop if reverse else hop
        return combine(
            state, jax.tree.map(lambda a: lax.dynamic_index_in_dim(a, source, 0, False), gathered)
        )

    return lax.fori_loop(0, ahead, one, state)


def summed_rows(portion, rows, axis):
    count = rows * lax.axis_size(axis)
    sent = portion(jnp.int32(0), count).astype(jnp.bfloat16)
    return lax.psum_scatter(sent, axis, scatter_dimension=0, tiled=True).astype(jnp.float32)


def combine_pair(earlier, latter):
    return (earlier[0] * latter[0], latter[0] * earlier[1] + latter[1])


def block_product(convolved, weight):
    blocks = weight.shape[0]
    block_width = weight.shape[1]
    grouped = convolved.reshape(convolved.shape[0], convolved.shape[1], blocks, block_width)
    product = jnp.einsum("slhi,hij->slhj", grouped, weight, preferred_element_type=jnp.float32)
    return product.reshape(convolved.shape)


def per_device(
    tokens,
    norm_gain,
    entry_projection,
    valve_projection,
    filter_taps,
    conv_bias,
    recur_weight,
    recur_bias,
    entry_weight,
    entry_bias,
    forget_rate,
    output_weight,
):
    widened = tokens.astype(jnp.float32)
    scaled = widened * lax.rsqrt(jnp.mean(widened * widened, axis=-1, keepdims=True) + epsilon)
    rescaled_values = (scaled * norm_gain).astype(jnp.bfloat16)
    channels = entry_projection.shape[1]

    def project(partition_lines, row_start):
        input_part = jnp.einsum(
            "tgy,yu->tgu", partition_lines, entry_projection, preferred_element_type=jnp.float32
        )
        gate_part = jnp.einsum(
            "tgy,yu->tgu", partition_lines, valve_projection, preferred_element_type=jnp.float32
        )
        return jnp.concatenate(
            [input_part.astype(jnp.bfloat16), gate_part.astype(jnp.bfloat16)], axis=-1
        )

    projected = over_all(rescaled_values, "tp", 1, project)
    conv_input = projected[:, :, :channels]
    gate_logits = projected[:, :, channels:]
    conv_width = filter_taps.shape[0]
    length = conv_input.shape[1]
    before = from_behind(conv_input[:, length - (conv_width - 1) :, :], "sp", 1)
    padded = jnp.concatenate([before, conv_input], axis=1).astype(jnp.float32)
    summed = conv_bias + padded[:, 0:length] * filter_taps[0]
    for offset in range(1, conv_width):
        summed = summed + padded[:, offset : offset + length] * filter_taps[offset]
    convolved = summed.astype(jnp.bfloat16)
    recur_gate = jax.nn.sigmoid(block_product(convolved, recur_weight) + recur_bias)
    entry_gate = jax.nn.sigmoid(block_product(convolved, entry_weight) + entry_bias)
    log_decay = -gate_power * recur_gate * forget_rate
    decay = jnp.exp(log_decay)
    pushed = jnp.sqrt(-jnp.expm1(2.0 * log_decay)) * (entry_gate * convolved.astype(jnp.float32))
    local_decay, local_state = lax.associative_scan(combine_pair, (decay, pushed), axis=1)
    stretch_decay = local_decay[:, -1]
    stretch_state = local_state[:, -1]
    unchanged_passthrough = (jnp.ones_like(stretch_decay), jnp.zeros_like(stretch_state))
    entering = entering_2(
        (stretch_decay, stretch_state), "sp", combine_pair, unchanged_passthrough, False
    )[1]
    hidden_state = local_state + local_decay * entering[:, None]
    valved_lines = (hidden_state * jax.nn.silu(gate_logits.astype(jnp.float32))).astype(
        jnp.bfloat16
    )
    kept_rows = length // lax.axis_size("tp")

    def output_term(row_start, row_count):
        segment = lax.dynamic_slice_in_dim(valved_lines, row_start, row_count, 1)
        return jnp.einsum("slc,cd->lsd", segment, output_weight, preferred_element_type=jnp.float32)

    mixed_rows = summed_rows(output_term, kept_rows, "tp")
    return jnp.transpose(mixed_rows.astype(jnp.bfloat16), (1, 0, 2))


def solution(mesh):
    return jax.shard_map(
        per_device,
        mesh=mesh,
        in_specs=(
            P(None, ("sp", "tp"), None),
            P(),
            P(None, "tp"),
            P(None, "tp"),
            P(None, "tp"),
            P("tp"),
            P("tp", None, None),
            P("tp"),
            P("tp", None, None),
            P("tp"),
            P("tp"),
            P("tp", None),
        ),
        out_specs=P(None, ("sp", "tp"), None),
        check_vma=False,
    )
```

profile of v0, /device:TPU:0, one launch (start us, length us, event | category | flops | bytes accessed | tf_op | source)
XLA Modules:
  0.0 261.2 jit_solution(6959251722430854535)
XLA Ops:
  7.9 2.0 fusion.2
  10.8 75.1 %all-gather.4.cloned.1.call-done = bf16[4,256,2048]{2,1,0:T(8,128)(2,1)} async-done(((bf16[4,32,2048]{2,1,0:T(8,128)(2,1)}), bf16[4,256,2048]{2,1,0:T(8,128)(2,1)}) %all-gather.4.cloned.1.call-update) | async-done | bytes 4194320 | tf_op jit(solution)/shard_map/all_gather | solution.py:11
  85.9 3.7 %convolution_convert_fusion.1 = bf16[4,256,256]{2,1,0:T(8,128)(2,1)S(1)} fusion(bf16[4,256,2048]{2,1,0:T(8,128)(2,1)} %all-gather.4.cloned.1.call-done, bf16[2048,256]{1,0:T(8,128)(2,1)} %param.16), kind=kOutput, calls=%fused_computation.10 | convolution fusion | flops 1074003968 | bytes 5767168 | tf_op jit(solution)/shard_map/tgy,yu->tgu/dot_general | solution.py:74
  92.5 1.4 convolution_bitcast_fusion
  93.8 2.3 copy.24
  96.1 3.1 %reshape.30 = f32[4,256,256]{2,1,0:T(8,128)} reshape(f32[4,256,2,128]{3,2,1,0:T(2,128)} %copy.24) | data formatting | bytes 2097152 | tf_op jit(solution)/shard_map/reshape | solution.py:51
  100.5 1.5 copy.21
  102.0 1.8 reshape.29
  103.9 3.1 %multiply_multiply_fusion = (f32[4,256,256]{2,1,0:T(8,128)S(1)}, f32[4,256,256]{2,1,0:T(8,128)S(1)}) fusion(f32[4,256,256]{2,1,0:T(8,128)} %reshape.30, f32[256]{0:T(256)S(1)} %copy-done.8, f32[256]{0:T(256)S(1)} %broadcast_multiply_fusion, f32[4,256,256]{2,1,0:T(8,128)} %reshape.29, f32[256]{0:T(256)S(1)} %copy-done.9, f32[256]{0:T(256)S(1)} %bitcast.83, ...), kind=kLoop, calls=%fused_computation.35 | loop fusion | flops 6029312 | bytes 8396800 | tf_op jit(solution)/shard_map/mul | solution.py:99
  108.0 3.3 %slice.330 = f32[4,127,256]{2,1,0:T(8,128)} slice(f32[4,256,256]{2,1,0:T(8,128)} %copy-done.1), slice={[0:4:1], [2:256:2], [0:256:1]} | slice | bytes 1040384 | tf_op jit(solution)/shard_map/slice | solution.py:100
  111.3 3.3 %slice.276 = f32[4,128,256]{2,1,0:T(8,128)} slice(f32[4,256,256]{2,1,0:T(8,128)} %copy-done.1), slice={[0:4:1], [1:256:2], [0:256:1]} | slice | bytes 1048576 | tf_op jit(solution)/shard_map/slice | solution.py:100
  114.5 3.3 %slice.275 = f32[4,128,256]{2,1,0:T(8,128)} slice(f32[4,256,256]{2,1,0:T(8,128)} %copy-done.1), slice={[0:4:1], [0:255:2], [0:256:1]} | slice | bytes 1048576 | tf_op jit(solution)/shard_map/slice | solution.py:100
  117.8 1.5 slice.278
  119.3 1.5 slice.274
  120.8 1.5 slice.273
  122.3 1.7 multiply_add_fusion
  131.1 2.2 fusion.23
  133.3 2.7 %pad.128 = f32[4,256,256]{2,1,0:T(8,128)} pad(f32[4,128,256]{2,1,0:T(8,128)S(1)} %pad_maximum_fusion.1, f32[]{:T(128)} %constant.30.clone.1), padding=0_0_0x0_1_1x0_0_0 | pad | bytes 1572868 | tf_op jit(solution)/shard_map/pad | solution.py:100
  137.1 2.6 %pad.112 = f32[4,256,256]{2,1,0:T(8,128)} pad(f32[4,128,256]{2,1,0:T(8,128)S(1)} %pad_maximum_fusion, f32[]{:T(128)} %constant.30.clone.1), padding=0_0_0x0_1_1x0_0_0 | pad | bytes 1572868 | tf_op jit(solution)/shard_map/pad | solution.py:100
  140.7 7.5 %all-gather.1 = f32[16,1,256]{2,1,0:T(1,128)S(1)} all-gather(f32[4,1,256]{2,1,0:T(1,128)S(1)} %slice_add_fusion), channel_id=3, replica_groups=mesh['sp'=4,'tp'=8] {'sp'}, dimensions={0}, use_global_device_ids=true | all-gather | bytes 20480 | tf_op jit(solution)/shard_map/all_gather | solution.py:24
  148.3 2.6 pad.129
  151.7 5.4 %all-gather = f32[16,1,256]{2,1,0:T(1,128)S(1)} all-gather(f32[4,1,256]{2,1,0:T(1,128)S(1)} %slice_add_fusion.1), channel_id=2, replica_groups=mesh['sp'=4,'tp'=8] {'sp'}, dimensions={0}, use_global_device_ids=true | all-gather | bytes 20480 | tf_op jit(solution)/shard_map/all_gather | solution.py:24
  157.4 9.9 %convert_bitcast_fusion = bf16[256,4,2048]{2,0,1:T(8,128)(2,1)} fusion(bf16[4,256,2048]{2,1,0:T(8,128)(2,1)} %all-gather.4.cloned.1.call-done, bf16[256,2048]{1,0:T(8,128)(2,1)S(1)} %copy-done, bf16[2048,256]{1,0:T(8,128)(2,1)} %param.17, f32[4,256,256]{2,1,0:T(8,128)} %pad.128, f32[4,256,256]{2,1,0:T(8,128)} %pad.129, f32[4,256,256]{2,1,0:T(8,128)} %pad.112, ...), kind=kOutput, calls=%fused_computation.2 | convolution fusion | flops 2152726528 | bytes 14684160 | tf_op jit(solution)/shard_map/slc,cd->lsd/dot_general | solution.py:115
  167.3 87.0 %reduce-scatter.2.cloned.1.call-done = bf16[32,4,2048]{2,0,1:T(8,128)(2,1)} async-done(((bf16[256,4,2048]{2,0,1:T(8,128)(2,1)}), bf16[32,4,2048]{2,0,1:T(8,128)(2,1)}) %reduce-scatter.2.cloned.1.call-update) | async-done | bytes 524304 | tf_op jit(solution)/shard_map/reduce_scatter | solution.py:39
  (154 shorter events, 17.0 us)
Async XLA Ops:
  6.5 150.9 %copy-start = (bf16[256,2048]{1,0:T(8,128)(2,1)S(1)}, bf16[256,2048]{1,0:T(8,128)(2,1)}, u32[]{:S(2)}) copy-start(bf16[256,2048]{1,0:T(8,128)(2,1)} %param.25) | copy-start | bytes 3145732
  6.5 79.4 %all-gather.4.cloned.1.call-start = ((), (), s32[]{:S(2)}) async-start(), calls=%async_computation.1 | async-start | bytes 4718592 | tf_op jit(solution)/shard_map/all_gather | solution.py:11
  9.9 81.1 %copy-start.10 = (f32[256]{0:T(256)S(1)}, f32[256]{0:T(256)}, u32[]{:S(2)}) copy-start(f32[256]{0:T(256)} %param.24) | copy-start | bytes 3076
  9.9 244.4 %reduce-scatter.2.cloned.1.call-start = ((), (), s32[]{:S(2)}) async-start(), calls=%async_computation.2 | async-start | bytes 4718592 | tf_op jit(solution)/shard_map/reduce_scatter | solution.py:39
  10.8 81.1 %copy-start.7 = (f32[256]{0:T(256)S(1)}, f32[256]{0:T(256)}, u32[]{:S(2)}) copy-start(f32[256]{0:T(256)} %param.19) | copy-start | bytes 3076
  89.6 2.8 %copy-start.5 = (bf16[2,128,128]{2,1,0:T(8,128)(2,1)S(1)}, bf16[2,128,128]{2,1,0:T(8,128)(2,1)}, u32[]{:S(2)}) copy-start(bf16[2,128,128]{2,1,0:T(8,128)(2,1)} %param.22) | copy-start | bytes 196612
  89.7 2.1 collective-permute-start
  91.9 7.3 %copy-start.6 = (bf16[2,128,128]{2,1,0:T(8,128)(2,1)S(1)}, bf16[2,128,128]{2,1,0:T(8,128)(2,1)}, u32[]{:S(2)}) copy-start(bf16[2,128,128]{2,1,0:T(8,128)(2,1)} %param.20) | copy-start | bytes 196612
  96.1 7.8 %copy-start.8 = (f32[256]{0:T(256)S(1)}, f32[256]{0:T(256)}, u32[]{:S(2)}) copy-start(f32[256]{0:T(256)} %param.23) | copy-start | bytes 3076
  96.1 7.8 %copy-start.9 = (f32[256]{0:T(256)S(1)}, f32[256]{0:T(256)}, u32[]{:S(2)}) copy-start(f32[256]{0:T(256)} %param.21) | copy-start | bytes 3076
  107.0 1.0 copy-start.1
  127.4 1.2 copy-start.4
  133.3 6.5 %copy-start.3 = (f32[4,128,256]{2,1,0:T(8,128)S(1)}, f32[4,128,256]{2,1,0:T(8,128)}, u32[]{:S(2)}) copy-start(f32[4,128,256]{2,1,0:T(8,128)} %add.263) | copy-start | bytes 1572868
  133.3 15.0 %copy-start.2 = (f32[4,128,256]{2,1,0:T(8,128)S(1)}, f32[4,128,256]{2,1,0:T(8,128)}, u32[]{:S(2)}) copy-start(f32[4,128,256]{2,1,0:T(8,128)} %add.272) | copy-start | bytes 1572868
Sparse Core Ops, SparseCore 0:
  10.0 75.8 all-gather.3
  167.4 86.8 reduce-scatter.1
where the time goes:
time: 262 us; the launch traced here: 261 us
  waiting for transfers between devices  163 us (62%)
  local copies, waits for them, and re-layouts  37 us (14%)
  other arithmetic  16.3 us (6%)
  matrix products  16.3 us (6%)
  between operations  14.2 us (5%)
  blocking collectives  12.9 us (5%)
    reduce_scatter x1, waiting for transfers between devices, summed_rows(): lax.psum_scatter(sent, axis, scatter_dimension=0, tiled=True)  87 us
    all_gather x1, waiting for transfers between devices, over_all(): return work(lax.all_gather(shard, axis, axis=dim, tiled=True), jnp.int32(0))  75.1 us
    slice x52, local copies, waits for them, and re-layouts, per_device(): lax.associative_scan(combine_pair, (decay, pushed), axis=1)  16.7 us
    all_gather x2, blocking collectives, entering_2(): gathered = jax.tree.map(lambda a: lax.all_gather(a, axis), part)  12.9 us
    dot_general x1, matrix products, output_term(): jnp.einsum('slc,cd->lsd', segment, output_weight, preferred_element_type=...  9.85 us
    pad x28, local copies, waits for them, and re-layouts, per_device(): lax.associative_scan(combine_pair, (decay, pushed), axis=1)  9.63 us
  transfers between devices with their start and end apart: 3, of which 3 were waited for; matrix products, arithmetic and copies ran while one was open for 0% of the time, Pallas kernels for 0%

commit v1 on v0

v1 whole, which is shorter than its diff:
```python
import functools

import jax
import jax.numpy as jnp
from jax import lax
from jax.experimental import pallas as pl
from jax.experimental.pallas import tpu as pltpu
from jax.sharding import PartitionSpec as P

epsilon = 1e-06
gate_power = 8.0
MESH = pl.DeviceIdType.MESH
CORES = 2


def kernel(
    SP, TP, Y,
    tok_ref, gain_ref, ew_hbm, vw_hbm, taps_ref, cb_ref, rw_ref, rb_ref, iw_ref, ib_ref, fr_ref, ow_hbm,
    out_ref,
    xg, wf, ew, vw, cbuf, logits, hbuf, dbuf, gbuf, ga, halo, carry,
    tok_send, tok_recv, w_send, wx_send, wc_send, w_recv, a_send, a_recv, c_send, c_recv,
    h_send, h_recv, local,
):
    Z, X = TP // Y, SP // CORES
    sp, tp = lax.axis_index("sp"), lax.axis_index("tp")
    z, y = tp // Y, tp % Y
    x, c = sp // CORES, sp % CORES
    S, T, D = tok_ref.shape
    R = S * T
    C = ew.shape[1]
    B = rw_ref.shape[1]
    K = taps_ref.shape[0]
    H = S * (K - 1)
    HP = halo.shape[0]
    PIECE = wf.shape[2]
    pending = []

    def go(pred, make):
        @pl.when(pred)
        def _():
            make().start()

        pending.append((pred, make))

    loads = [
        pltpu.make_async_copy(ew_hbm, ew, local.at[0]),
        pltpu.make_async_copy(vw_hbm, vw, local.at[1]),
    ]
    for q in range(SP):
        loads.append(
            pltpu.make_async_copy(ow_hbm.at[pl.ds(q * PIECE, PIECE)], wf.at[tp, q], local.at[2 + q])
        )
    for load in loads:
        load.start()

    barrier = pltpu.get_barrier_semaphore()
    for k in range(1, TP):
        pl.semaphore_signal(barrier, inc=1, device_id={"tp": (tp + k) % TP}, device_id_type=MESH)
    for k in range(1, SP):
        pl.semaphore_signal(barrier, inc=1, device_id={"sp": (sp + k) % SP}, device_id_type=MESH)

    r_i = lax.broadcasted_iota(jnp.int32, (R, R), 0)
    c_i = lax.broadcasted_iota(jnp.int32, (R, R), 1)
    to_time = jnp.where(c_i == (r_i % S) * T + r_i // S, 1.0, 0.0).astype(jnp.bfloat16)
    to_seq = jnp.where(r_i == (c_i % S) * T + c_i // S, 1.0, 0.0).astype(jnp.bfloat16)

    wide = tok_ref[...].reshape(R, D).astype(jnp.float32)
    scaled = wide * lax.rsqrt(jnp.mean(wide * wide, axis=-1, keepdims=True) + epsilon)
    normed = (scaled * gain_ref[...]).astype(jnp.bfloat16)
    xg[tp] = jnp.dot(to_time, normed, preferred_element_type=jnp.float32).astype(jnp.bfloat16)

    pl.semaphore_wait(barrier, TP - 1 + SP - 1)

    def tok_copy(slot, target, way):
        return pltpu.make_async_remote_copy(
            xg.at[slot], xg.at[slot], tok_send.at[slot, way], tok_recv.at[slot],
            device_id={"tp": target}, device_id_type=MESH)

    def w_copy(slot, target, way):
        return pltpu.make_async_remote_copy(
            wf.at[slot, sp], wf.at[slot, sp], w_send.at[slot, way], w_recv.at[slot, sp],
            device_id={"tp": target}, device_id_type=MESH)

    def x_copy(slot, xx, step, way):
        q = xx * CORES + c
        return pltpu.make_async_remote_copy(
            wf.at[slot, q], wf.at[slot, q], wx_send.at[slot, xx, way], w_recv.at[slot, q],
            device_id={"sp": sp + step * CORES}, device_id_type=MESH)

    def core_copy(slot, xx):
        q = xx * CORES + c
        return pltpu.make_async_remote_copy(
            wf.at[slot, q], wf.at[slot, q], wc_send.at[slot, xx], w_recv.at[slot, q],
            device_id={"sp": x * CORES + 1 - c}, device_id_type=MESH)

    def project(slot):
        a = xg[slot]
        base = pl.multiple_of(slot * R + HP, 16)
        cin = jnp.dot(a, ew[...], preferred_element_type=jnp.float32)
        cbuf[pl.ds(base, R), :] = cin.astype(jnp.bfloat16).astype(jnp.float32)
        lg = jnp.dot(a, vw[...], preferred_element_type=jnp.float32)
        logits[slot] = lg.astype(jnp.bfloat16)

    def inside(v, n):
        return (v >= 0) & (v < n)

    def spread(copy, slot, valid, zz_step, both):
        for way, step in ((0, 1), (1, -1)):
            if both or step == zz_step:
                go(valid & inside(z + step, Z), functools.partial(copy, slot, tp + step * Y, way))
        for way, step in ((2, 1), (3, -1)):
            go(valid & inside(y + step, Y), functools.partial(copy, slot, tp + step, way))

    def received(buf_at, sem):
        pltpu.make_async_copy(buf_at, buf_at, sem).wait()

    spread(tok_copy, tp, z >= 0, 0, True)
    loads[0].wait()
    loads[1].wait()
    for q in range(SP):
        loads[2 + q].wait()

    def x_spread(slot, valid):
        for way, step in ((0, 1), (1, -1)):
            go(valid & inside(x + step, X), functools.partial(x_copy, slot, x, step, way))
        go(valid, functools.partial(core_copy, slot, x))

    project(tp)

    def along_z(d, copy, arrived, after):
        for step in (1, -1):
            zz = z - step * d
            valid = inside(zz, Z)
            slot = zz * Y + y

            @pl.when(valid)
            def _(slot=slot):
                arrived(slot)

            spread(copy, slot, valid, step, False)
            after(slot, valid)

    def along_y(copy, arrived, after):
        for e in range(1, Y):
            for d in range(Z):
                for zs in (1, -1) if d else (1,):
                    for step in (1, -1):
                        zz, yy = z - zs * d, y - step * e
                        valid = inside(zz, Z) & inside(yy, Y)
                        slot = zz * Y + yy

                        @pl.when(valid)
                        def _(slot=slot):
                            arrived(slot)

                        go(
                            valid & inside(y + step, Y),
                            functools.partial(copy, slot, tp + step, 2 if step == 1 else 3),
                        )
                        after(slot, valid)

    def tok_arrived(slot):
        received(xg.at[slot], tok_recv.at[slot])

    def tok_after(slot, valid):
        @pl.when(valid)
        def _():
            project(slot)

    def w_arrived(slot):
        received(wf.at[slot, sp], w_recv.at[slot, sp])

    for d in range(1, Z):
        along_z(d, tok_copy, tok_arrived, tok_after)
    spread(w_copy, tp, z >= 0, 0, True)
    for d in range(1, Z - 1):
        along_z(d, w_copy, w_arrived, x_spread)
    along_y(tok_copy, tok_arrived, tok_after)

    def halo_copy():
        return pltpu.make_async_remote_copy(
            cbuf.at[pl.ds(TP * R, HP)], halo, h_send, h_recv,
            device_id={"sp": sp + 1}, device_id_type=MESH)

    go(sp + 1 < SP, halo_copy)

    @pl.when(sp == 0)
    def _():
        cbuf[pl.ds(0, HP), :] = jnp.zeros((HP, C), jnp.float32)

    @pl.when(sp > 0)
    def _():
        received(halo, h_recv)
        cbuf[pl.ds(0, HP), :] = halo[...]

    def spreadrows(v):
        return jnp.broadcast_to(
            jnp.concatenate([v] * (8 // S), axis=0)[None], (R // 8, 8, B)
        ).reshape(R, B)

    for b in range(C // B):
        cols = slice(b * B, (b + 1) * B)

        def chunk(j, state, b=b, cols=cols):
            dc, hc = state
            blk = cbuf[pl.ds(pl.multiple_of(j * R, 16), R + HP), cols]
            conv = cb_ref[:, cols]
            for k in range(K):
                o = HP - H + S * k
                conv = conv + blk[o : o + R] * taps_ref[k : k + 1, cols]
            cv = conv.astype(jnp.bfloat16)
            rg = jax.nn.sigmoid(
                jnp.dot(cv, rw_ref[b], preferred_element_type=jnp.float32) + rb_ref[:, cols])
            ig = jax.nn.sigmoid(
                jnp.dot(cv, iw_ref[b], preferred_element_type=jnp.float32) + ib_ref[:, cols])
            ld = -gate_power * rg * fr_ref[:, cols]
            a = jnp.exp(ld)
            v = jnp.sqrt(-jnp.tanh(ld) * (a * a + 1.0)) * (ig * cv.astype(jnp.float32))
            d = S
            while d < R:
                a_s = jnp.concatenate([jnp.ones((d, B), jnp.float32), a[: R - d]], axis=0)
                v_s = jnp.concatenate([jnp.zeros((d, B), jnp.float32), v[: R - d]], axis=0)
                v = a * v_s + v
                a = a * a_s
                d *= 2
            v = v + a * spreadrows(hc)
            a = a * spreadrows(dc)
            hbuf[j, :, cols] = v
            dbuf[j, :, cols] = a
            return a[R - S :], v[R - S :]

        dc, hc = lax.fori_loop(
            0, TP, chunk, (jnp.ones((S, B), jnp.float32), jnp.zeros((S, B), jnp.float32)))
        carry[sp, 0, :, cols] = dc
        carry[sp, 1, :, cols] = hc

    def carry_copy(k):
        return pltpu.make_async_remote_copy(
            carry.at[sp], carry.at[sp], c_send.at[k], c_recv.at[sp],
            device_id={"sp": (sp + k) % SP}, device_id_type=MESH)

    for k in range(1, SP):
        go(sp >= 0, functools.partial(carry_copy, k))
    if Z > 1:
        along_z(Z - 1, w_copy, w_arrived, x_spread)
    for k in range(1, SP):
        other = (sp + k) % SP
        received(carry.at[other], c_recv.at[other])
    entering = jnp.zeros((S, C), jnp.float32)
    for k in range(SP - 1):
        entering = jnp.where(k < sp, carry[k, 0] * entering + carry[k, 1], entering)

    rows = jnp.broadcast_to(
        jnp.concatenate([entering] * (8 // S), axis=0)[None], (R // 8, 8, C)
    ).reshape(R, C)

    def gate(j):
        h = hbuf[j] + dbuf[j] * rows
        g = logits[j].astype(jnp.float32)
        gated = (h * (g / (1.0 + jnp.exp(-g)))).astype(jnp.bfloat16)
        return jnp.dot(to_seq, gated, preferred_element_type=jnp.float32).astype(jnp.bfloat16)

    def a_copy(k):
        target = (tp + k) % TP
        return pltpu.make_async_remote_copy(
            gbuf.at[target], ga.at[tp], a_send.at[k], a_recv.at[tp],
            device_id={"tp": target}, device_id_type=MESH)

    for k in range(1, TP):
        j = (tp + k) % TP
        gbuf[j] = gate(j)
        go(tp >= 0, functools.partial(a_copy, k))
    ga[tp] = gate(tp)

    along_y(w_copy, w_arrived, x_spread)

    for k in range(1, TP):
        i = (tp + k) % TP
        for d in range(1, X):
            for step in (1, -1):
                xx = x - step * d
                valid = inside(xx, X)
                q = xx * CORES + c

                @pl.when(valid)
                def _(i=i, q=q):
                    received(wf.at[i, q], w_recv.at[i, q])

                go(
                    valid & inside(x + step, X),
                    functools.partial(x_copy, i, xx, step, 0 if step == 1 else 1),
                )
                go(valid, functools.partial(core_copy, i, xx))
    for k in range(1, TP):
        i = (tp + k) % TP
        for xx in range(X):
            q = xx * CORES + 1 - c
            received(wf.at[i, q], w_recv.at[i, q])

    for k in range(1, TP):
        other = (tp + k) % TP
        received(ga.at[other], a_recv.at[other])

    tile = 512 if D % 512 == 0 else D
    for n in range(D // tile):
        at = slice(n * tile, (n + 1) * tile)
        acc = jnp.zeros((R, tile), jnp.float32)
        for i in range(TP):
            acc = acc + jnp.dot(
                ga[i], wf[i, :, :, at].reshape(C, tile), preferred_element_type=jnp.float32)
        out_ref[:, :, at] = acc.astype(jnp.bfloat16).reshape(S, T, tile)

    for pred, make in pending:

        @pl.when(pred)
        def _(make=make):
            make().wait_send()


def per_device(
    SP, TP, Y,
    tokens, norm_gain, entry_projection, valve_projection, filter_taps, conv_bias,
    recur_weight, recur_bias, entry_weight, entry_bias, forget_rate, output_weight,
):
    S, T, D = tokens.shape
    R = S * T
    C = entry_projection.shape[1]
    HP = 16
    vmem = pl.BlockSpec(memory_space=pltpu.VMEM)
    hbm = pl.BlockSpec(memory_space=pl.ANY)
    f32, bf16 = jnp.float32, jnp.bfloat16
    dma = pltpu.SemaphoreType.DMA
    X = SP // CORES
    return pl.pallas_call(
        functools.partial(kernel, SP, TP, Y),
        out_shape=jax.ShapeDtypeStruct(tokens.shape, bf16),
        in_specs=[vmem, vmem, hbm, hbm] + [vmem] * 7 + [hbm],
        out_specs=vmem,
        scratch_shapes=[
            pltpu.VMEM((TP, R, D), bf16),
            pltpu.VMEM((TP, SP, C // SP, D), bf16),
            pltpu.VMEM((D, C), bf16),
            pltpu.VMEM((D, C), bf16),
            pltpu.VMEM((TP * R + HP, C), f32),
            pltpu.VMEM((TP, R, C), bf16),
            pltpu.VMEM((TP, R, C), f32),
            pltpu.VMEM((TP, R, C), f32),
            pltpu.VMEM((TP, R, C), bf16),
            pltpu.VMEM((TP, R, C), bf16),
            pltpu.VMEM((HP, C), f32),
            pltpu.VMEM((SP, 2, S, C), f32),
            dma((TP, 4)), dma((TP,)),
            dma((TP, 4)), dma((TP, X, 2)), dma((TP, X)), dma((TP, SP)),
            dma((TP,)), dma((TP,)), dma((SP,)), dma((SP,)),
            dma, dma, dma((2 + SP,)),
        ],
        compiler_params=pltpu.CompilerParams(
            collective_id=0, has_side_effects=True, vmem_limit_bytes=60 * 1024 * 1024
        ),
    )(
        tokens, norm_gain[None], entry_projection, valve_projection, filter_taps, conv_bias[None],
        recur_weight, recur_bias[None], entry_weight, entry_bias[None], forget_rate[None],
        output_weight,
    )


def solution(mesh):
    SP, TP = mesh.shape["sp"], mesh.shape["tp"]
    try:
        Y = len({tuple(d.coords)[1] for d in mesh.devices.flat})
    except AttributeError:
        Y = 1
    return jax.shard_map(
        functools.partial(per_device, SP, TP, Y),
        mesh=mesh,
        in_specs=(
            P(None, ("sp", "tp"), None),
            P(),
            P(None, "tp"),
            P(None, "tp"),
            P(None, "tp"),
            P("tp"),
            P("tp", None, None),
            P("tp"),
            P("tp", None, None),
            P("tp"),
            P("tp"),
            P("tp", None),
        ),
        out_specs=P(None, ("sp", "tp"), None),
        check_vma=False,
    )
```

time: 262 us -> 104 us (0.40)
  waiting for transfers between devices: 163 us -> 0 us
  Pallas kernels: 0 us -> 102 us
  local copies, waits for them, and re-layouts: 37 us -> 1.88 us
  matrix products: 16.3 us -> 0 us
  other arithmetic: 16.3 us -> 0 us
  between operations: 14.2 us -> 0.01 us
  blocking collectives: 12.9 us -> 0 us
    pallas_call x0 -> x1, Pallas kernels: none -> 102 us  [per_device(): pl.pallas_call(functools.partial(kernel, SP, TP, Y), out_shape=jax.ShapeD...]
    reduce_scatter x1 -> x0, waiting for transfers between devices: 87 us -> none  [summed_rows(): lax.psum_scatter(sent, axis, scatter_dimension=0, tiled=True)]
    all_gather x1 -> x0, waiting for transfers between devices: 75.1 us -> none  [over_all(): return work(lax.all_gather(shard, axis, axis=dim, tiled=True), jnp.int32(0))]
    slice x54 -> x0, local copies, waits for them, and re-layouts: 17.6 us -> none  [the longest x52 16.7 us: per_device(): lax.associative_scan(combine_pair, (decay, pushed), axis=1)]
    dot_general x4 -> x0, matrix products: 16.3 us -> none  [the longest x1 9.85 us: output_term(): jnp.einsum('slc,cd->lsd', segment, output_weight, preferred_element_type=...]
    all_gather x2 -> x0, blocking collectives: 12.9 us -> none  [entering_2(): gathered = jax.tree.map(lambda a: lax.all_gather(a, axis), part)]
    pad x28 -> x0, local copies, waits for them, and re-layouts: 9.63 us -> none  [per_device(): lax.associative_scan(combine_pair, (decay, pushed), axis=1)]
    add x28 -> x0, other arithmetic: 7.73 us -> none  [the longest x13 4.26 us: combine_pair(): return (earlier[0] * latter[0], latter[0] * earlier[1] + latter[1])]
  transfers between devices with their start and end apart: 3 -> 0, of which waited for: 3 -> 0; matrix products, arithmetic and copies ran while one was open for 0% -> 0% of each run, Pallas kernels for 0% -> 0%
where the time goes in v1:
time: 104 us; the launch traced here: 103 us
  Pallas kernels  102 us (98%)
  local copies, waits for them, and re-layouts  1.88 us (2%)
    pallas_call x1, Pallas kernels, per_device(): pl.pallas_call(functools.partial(kernel, SP, TP, Y), out_shape=jax.ShapeD...  102 us

profile of v1, /device:TPU:0, one launch (start us, length us, event | category | flops | bytes accessed | tf_op | source)
XLA Modules:
  0.0 103.4 jit_solution(5438374081550396176)
XLA Ops:
  0.0 101.5 %shard_map.118 = bf16[4,32,2048]{2,1,0:T(8,128)(2,1)} custom-call(bf16[4,32,2048]{2,1,0:T(8,128)(2,1)} %tok_ref.1, f32[1,2048]{1,0:T(1,128)} %bitcast.5, bf16[2048,256]{1,0:T(8,128)(2,1)} %ew_hbm.1, bf16[2048,256]{1,0:T(8,128)(2,1)} %vw_hbm.1, f32[4,256]{1,0:T(4,128)} %taps_ref.1, f32[1,256]{1,0:T(1,128)} %bitcast.6, bf16[2,128,128]{2,1,0:T(8,128)(2,1)} %rw_ref.1, ...), custom_call_target="tpu_custom_call" | custom-call | tf_op jit(solution)/shard_map/pallas_call | solution.py:334
  101.5 1.9 %copy.14 = bf16[4,32,2048]{2,1,0:T(8,128)(2,1)} copy(bf16[4,32,2048]{2,1,0:T(8,128)(2,1)} %shard_map.118) | data formatting | bytes 1048576

commit v2 on v1

--- a/solution.py
+++ b/solution.py
@@ -19,7 +19,7 @@
     out_ref,
     xg, wf, ew, vw, cbuf, logits, hbuf, dbuf, gbuf, ga, halo, carry,
     tok_send, tok_recv, w_send, wx_send, wc_send, w_recv, a_send, a_recv, c_send, c_recv,
-    h_send, h_recv, local,
+    h_send, h_recv, p_send, p_recv, local, pbuf, rbuf,
 ):
     Z, X = TP // Y, SP // CORES
     sp, tp = lax.axis_index("sp"), lax.axis_index("tp")
@@ -48,7 +48,7 @@
     ]
     for q in range(SP):
         loads.append(
-            pltpu.make_async_copy(ow_hbm.at[pl.ds(q * PIECE, PIECE)], wf.at[tp, q], local.at[2 + q])
+            pltpu.make_async_copy(ow_hbm.at[pl.ds(q * PIECE, PIECE)], wf.at[z, q], local.at[2 + q])
         )
     for load in loads:
         load.start()
@@ -104,78 +104,85 @@
     def inside(v, n):
         return (v >= 0) & (v < n)
 
-    def spread(copy, slot, valid, zz_step, both):
-        for way, step in ((0, 1), (1, -1)):
-            if both or step == zz_step:
-                go(valid & inside(z + step, Z), functools.partial(copy, slot, tp + step * Y, way))
+    def pass_z(copy, slot, valid, step):
+        way = 0 if step == 1 else 1
+        go(valid & inside(z + step, Z), functools.partial(copy, slot, tp + step * Y, way))
+
+    def pass_y(slot, valid):
         for way, step in ((2, 1), (3, -1)):
-            go(valid & inside(y + step, Y), functools.partial(copy, slot, tp + step, way))
+            go(valid & inside(y + step, Y), functools.partial(tok_copy, slot, tp + step, way))
 
     def received(buf_at, sem):
         pltpu.make_async_copy(buf_at, buf_at, sem).wait()
 
-    spread(tok_copy, tp, z >= 0, 0, True)
-    loads[0].wait()
-    loads[1].wait()
-    for q in range(SP):
-        loads[2 + q].wait()
+    for step in (1, -1):
+        pass_z(tok_copy, tp, z >= 0, step)
+    pass_y(tp, z >= 0)
+    for load in loads:
+        load.wait()
+    project(tp)
+
+    def own_piece(d):
+        pass_z(w_copy, z, z == d, 1)
+        pass_z(w_copy, z, Z - 1 - z == d, -1)
+
+    own_piece(0)
 
     def x_spread(slot, valid):
         for way, step in ((0, 1), (1, -1)):
             go(valid & inside(x + step, X), functools.partial(x_copy, slot, x, step, way))
         go(valid, functools.partial(core_copy, slot, x))
 
-    project(tp)
-
-    def along_z(d, copy, arrived, after):
+    def along_z(d, copy, slot_of, arrived, after):
         for step in (1, -1):
             zz = z - step * d
             valid = inside(zz, Z)
-            slot = zz * Y + y
+            slot = slot_of(zz)
 
             @pl.when(valid)
             def _(slot=slot):
                 arrived(slot)
 
-            spread(copy, slot, valid, step, False)
+            pass_z(copy, slot, valid, step)
             after(slot, valid)
-
-    def along_y(copy, arrived, after):
-        for e in range(1, Y):
-            for d in range(Z):
-                for zs in (1, -1) if d else (1,):
-                    for step in (1, -1):
-                        zz, yy = z - zs * d, y - step * e
-                        valid = inside(zz, Z) & inside(yy, Y)
-                        slot = zz * Y + yy
-
-                        @pl.when(valid)
-                        def _(slot=slot):
-                            arrived(slot)
-
-                        go(
-                            valid & inside(y + step, Y),
-                            functools.partial(copy, slot, tp + step, 2 if step == 1 else 3),
-                        )
-                        after(slot, valid)
 
     def tok_arrived(slot):
         received(xg.at[slot], tok_recv.at[slot])
 
-    def tok_after(slot, valid):
+    def tok_project(slot, valid):
         @pl.when(valid)
         def _():
             project(slot)
 
+    def tok_after(slot, valid):
+        pass_y(slot, valid)
+        tok_project(slot, valid)
+
     def w_arrived(slot):
         received(wf.at[slot, sp], w_recv.at[slot, sp])
 
     for d in range(1, Z):
-        along_z(d, tok_copy, tok_arrived, tok_after)
-    spread(w_copy, tp, z >= 0, 0, True)
+        along_z(d, tok_copy, lambda zz: zz * Y + y, tok_arrived, tok_after)
+        own_piece(d)
     for d in range(1, Z - 1):
-        along_z(d, w_copy, w_arrived, x_spread)
-    along_y(tok_copy, tok_arrived, tok_after)
+        along_z(d, w_copy, lambda zz: zz, w_arrived, x_spread)
+    for e in range(1, Y):
+        for d in range(Z):
+            for zs in (1, -1) if d else (1,):
+                for step in (1, -1):
+                    zz, yy = z - zs * d, y - step * e
+                    valid = inside(zz, Z) & inside(yy, Y)
+                    slot = zz * Y + yy
+
+                    @pl.when(valid)
+                    def _(slot=slot):
+                        tok_arrived(slot)
+
+                    go(
+                        valid & inside(y + step, Y),
+                        functools.partial(tok_copy, slot, tp + step, 2 if step == 1 else 3),
+                    )
+                    tok_project(slot, valid)
 
     def halo_copy():
         return pltpu.make_async_remote_copy(
@@ -242,7 +249,7 @@
     for k in range(1, SP):
         go(sp >= 0, functools.partial(carry_copy, k))
     if Z > 1:
-        along_z(Z - 1, w_copy, w_arrived, x_spread)
+        along_z(Z - 1, w_copy, lambda zz: zz, w_arrived, x_spread)
     for k in range(1, SP):
         other = (sp + k) % SP
         received(carry.at[other], c_recv.at[other])
@@ -261,21 +268,21 @@
         return jnp.dot(to_seq, gated, preferred_element_type=jnp.float32).astype(jnp.bfloat16)
 
     def a_copy(k):
-        target = (tp + k) % TP
-        return pltpu.make_async_remote_copy(
-            gbuf.at[target], ga.at[tp], a_send.at[k], a_recv.at[tp],
-            device_id={"tp": target}, device_id_type=MESH)
-
-    for k in range(1, TP):
-        j = (tp + k) % TP
-        gbuf[j] = gate(j)
-        go(tp >= 0, functools.partial(a_copy, k))
-    ga[tp] = gate(tp)
-
-    along_y(w_copy, w_arrived, x_spread)
-
-    for k in range(1, TP):
-        i = (tp + k) % TP
+        target = (z + k) % Z
+        return pltpu.make_async_remote_copy(
+            gbuf.at[pl.ds(target * Y, Y)], ga.at[z], a_send.at[k], a_recv.at[z],
+            device_id={"tp": target * Y + y}, device_id_type=MESH)
+
+    for k in range(1, Z):
+        for yy in range(Y):
+            j = (z + k) % Z * Y + yy
+            gbuf[j] = gate(j)
+        go(z >= 0, functools.partial(a_copy, k))
+    for yy in range(Y):
+        ga[z, yy] = gate(z * Y + yy)
+
+    for k in range(1, Z):
+        i = (z + k) % Z
         for d in range(1, X):
             for step in (1, -1):
                 xx = x - step * d
@@ -291,24 +298,43 @@
                     functools.partial(x_copy, i, xx, step, 0 if step == 1 else 1),
                 )
                 go(valid, functools.partial(core_copy, i, xx))
-    for k in range(1, TP):
-        i = (tp + k) % TP
+    for k in range(1, Z):
+        i = (z + k) % Z
         for xx in range(X):
             q = xx * CORES + 1 - c
             received(wf.at[i, q], w_recv.at[i, q])
 
-    for k in range(1, TP):
-        other = (tp + k) % TP
+    for k in range(1, Z):
+        other = (z + k) % Z
         received(ga.at[other], a_recv.at[other])
 
-    tile = 512 if D % 512 == 0 else D
-    for n in range(D // tile):
+    tile = pbuf.shape[3]
+    tiles = D // tile
+
+    def line_sum(yy, n):
         at = slice(n * tile, (n + 1) * tile)
         acc = jnp.zeros((R, tile), jnp.float32)
-        for i in range(TP):
+        for i in range(Z):
             acc = acc + jnp.dot(
-                ga[i], wf[i, :, :, at].reshape(C, tile), preferred_element_type=jnp.float32)
-        out_ref[:, :, at] = acc.astype(jnp.bfloat16).reshape(S, T, tile)
+                ga[i, yy], wf[i, :, :, at].reshape(C, tile), preferred_element_type=jnp.float32)
+        return acc
+
+    def p_copy(k, n):
+        return pltpu.make_async_remote_copy(
+            pbuf.at[k, n], rbuf.at[k, n], p_send.at[k, n], p_recv.at[k, n],
+            device_id={"tp": z * Y + (y + k) % Y}, device_id_type=MESH)
+
+    for n in range(tiles):
+        for k in range(1, Y):
+            pbuf[k, n] = line_sum((y + k) % Y, n).astype(jnp.bfloat16)
+            go(z >= 0, functools.partial(p_copy, k, n))
+    own = [line_sum(y, n) for n in range(tiles)]
+    for n in range(tiles):
+        total = own[n]
+        for k in range(1, Y):
+            received(rbuf.at[k, n], p_recv.at[k, n])
+            total = total + rbuf[k, n].astype(jnp.float32)
+        out_ref[:, :, n * tile : (n + 1) * tile] = total.astype(jnp.bfloat16).reshape(S, T, tile)
 
     for pred, make in pending:
 
@@ -330,7 +356,8 @@
     hbm = pl.BlockSpec(memory_space=pl.ANY)
     f32, bf16 = jnp.float32, jnp.bfloat16
     dma = pltpu.SemaphoreType.DMA
-    X = SP // CORES
+    X, Z = SP // CORES, TP // Y
+    tile = 512 if D % 512 == 0 else D
     return pl.pallas_call(
         functools.partial(kernel, SP, TP, Y),
         out_shape=jax.ShapeDtypeStruct(tokens.shape, bf16),
@@ -338,7 +365,7 @@
         out_specs=vmem,
         scratch_shapes=[
             pltpu.VMEM((TP, R, D), bf16),
-            pltpu.VMEM((TP, SP, C // SP, D), bf16),
+            pltpu.VMEM((Z, SP, C // SP, D), bf16),
             pltpu.VMEM((D, C), bf16),
             pltpu.VMEM((D, C), bf16),
             pltpu.VMEM((TP * R + HP, C), f32),
@@ -346,13 +373,15 @@
             pltpu.VMEM((TP, R, C), f32),
             pltpu.VMEM((TP, R, C), f32),
             pltpu.VMEM((TP, R, C), bf16),
-            pltpu.VMEM((TP, R, C), bf16),
+            pltpu.VMEM((Z, Y, R, C), bf16),
             pltpu.VMEM((HP, C), f32),
             pltpu.VMEM((SP, 2, S, C), f32),
             dma((TP, 4)), dma((TP,)),
-            dma((TP, 4)), dma((TP, X, 2)), dma((TP, X)), dma((TP, SP)),
-            dma((TP,)), dma((TP,)), dma((SP,)), dma((SP,)),
-            dma, dma, dma((2 + SP,)),
+            dma((Z, 2)), dma((Z, X, 2)), dma((Z, X)), dma((Z, SP)),
+            dma((Z,)), dma((Z,)), dma((SP,)), dma((SP,)),
+            dma, dma, dma((Y, D // tile)), dma((Y, D // tile)), dma((2 + SP,)),
+            pltpu.VMEM((Y, D // tile, R, tile), bf16),
+            pltpu.VMEM((Y, D // tile, R, tile), bf16),
         ],
         compiler_params=pltpu.CompilerParams(
             collective_id=0, has_side_effects=True, vmem_limit_bytes=60 * 1024 * 1024

time: 104 us -> 92.9 us (0.89)
  the two profiles are of different devices: /device:TPU:0 before, /device:TPU:24 now
where the time goes in v2:
time: 92.9 us; the launch traced here: 92.8 us
  Pallas kernels  90.9 us (98%)
  local copies, waits for them, and re-layouts  1.88 us (2%)
    pallas_call x1, Pallas kernels, per_device(): pl.pallas_call(functools.partial(kernel, SP, TP, Y), out_shape=jax.ShapeD...  90.9 us
    unnamed x1, local copies, waits for them, and re-layouts  1.88 us

profile of v2, /device:TPU:24, one launch (start us, length us, event | category | flops | bytes accessed | tf_op | source)
XLA Modules:
  0.0 92.8 jit_solution(11407852171992475291)
XLA Ops:
  0.0 90.9 %shard_map.118 = bf16[4,32,2048]{2,1,0:T(8,128)(2,1)} custom-call(bf16[4,32,2048]{2,1,0:T(8,128)(2,1)} %tok_ref.1, f32[1,2048]{1,0:T(1,128)} %bitcast.5, bf16[2048,256]{1,0:T(8,128)(2,1)} %ew_hbm.1, bf16[2048,256]{1,0:T(8,128)(2,1)} %vw_hbm.1, f32[4,256]{1,0:T(4,128)} %taps_ref.1, f32[1,256]{1,0:T(1,128)} %bitcast.6, bf16[2,128,128]{2,1,0:T(8,128)(2,1)} %rw_ref.1, ...), custom_call_target="tpu_custom_call" | custom-call | tf_op jit(solution)/shard_map/pallas_call | solution.py:361
  90.9 1.9 %copy.14 = bf16[4,32,2048]{2,1,0:T(8,128)(2,1)} copy(bf16[4,32,2048]{2,1,0:T(8,128)(2,1)} %shard_map.118) | data formatting | bytes 1048576

commit v3 on v2

--- a/solution.py
+++ b/solution.py
@@ -267,17 +267,18 @@
         gated = (h * (g / (1.0 + jnp.exp(-g)))).astype(jnp.bfloat16)
         return jnp.dot(to_seq, gated, preferred_element_type=jnp.float32).astype(jnp.bfloat16)
 
-    def a_copy(k):
+    def a_copy(k, e):
         target = (z + k) % Z
-        return pltpu.make_async_remote_copy(
-            gbuf.at[pl.ds(target * Y, Y)], ga.at[z], a_send.at[k], a_recv.at[z],
+        row = (y + e) % Y
+        return pltpu.make_async_remote_copy(
+            gbuf.at[target * Y + row], ga.at[z, row], a_send.at[k, e], a_recv.at[z, e],
             device_id={"tp": target * Y + y}, device_id_type=MESH)
 
-    for k in range(1, Z):
-        for yy in range(Y):
-            j = (z + k) % Z * Y + yy
+    for e in [*range(1, Y), 0]:
+        for k in range(1, Z):
+            j = (z + k) % Z * Y + (y + e) % Y
             gbuf[j] = gate(j)
-        go(z >= 0, functools.partial(a_copy, k))
+            go(z >= 0, functools.partial(a_copy, k, e))
     for yy in range(Y):
         ga[z, yy] = gate(z * Y + yy)
 
@@ -304,9 +305,13 @@
             q = xx * CORES + 1 - c
             received(wf.at[i, q], w_recv.at[i, q])
 
-    for k in range(1, Z):
-        other = (z + k) % Z
-        received(ga.at[other], a_recv.at[other])
+    def gated_arrived(e):
+        for k in range(1, Z):
+            other = (z + k) % Z
+            received(ga.at[other, (y + e) % Y], a_recv.at[other, e])
+
+    for e in range(1, Y):
+        gated_arrived(e)
 
     tile = pbuf.shape[3]
     tiles = D // tile
@@ -328,6 +333,7 @@
         for k in range(1, Y):
             pbuf[k, n] = line_sum((y + k) % Y, n).astype(jnp.bfloat16)
             go(z >= 0, functools.partial(p_copy, k, n))
+    gated_arrived(0)
     own = [line_sum(y, n) for n in range(tiles)]
     for n in range(tiles):
         total = own[n]
@@ -378,7 +384,7 @@
             pltpu.VMEM((SP, 2, S, C), f32),
             dma((TP, 4)), dma((TP,)),
             dma((Z, 2)), dma((Z, X, 2)), dma((Z, X)), dma((Z, SP)),
-            dma((Z,)), dma((Z,)), dma((SP,)), dma((SP,)),
+            dma((Z, Y)), dma((Z, Y)), dma((SP,)), dma((SP,)),
             dma, dma, dma((Y, D // tile)), dma((Y, D // tile)), dma((2 + SP,)),
             pltpu.VMEM((Y, D // tile, R, tile), bf16),
             pltpu.VMEM((Y, D // tile, R, tile), bf16),

time: 92.9 us -> 91.1 us (0.981)
  the two profiles are of different devices: /device:TPU:24 before, /device:TPU:0 now
where the time goes in v3:
time: 91.1 us; the launch traced here: 91 us
  Pallas kernels  89.1 us (98%)
  local copies, waits for them, and re-layouts  1.88 us (2%)
    pallas_call x1, Pallas kernels, per_device(): pl.pallas_call(functools.partial(kernel, SP, TP, Y), out_shape=jax.ShapeD...  89.1 us
    unnamed x1, local copies, waits for them, and re-layouts  1.88 us

profile of v3, /device:TPU:0, one launch (start us, length us, event | category | flops | bytes accessed | tf_op | source)
XLA Modules:
  0.0 91.0 jit_solution(7896200088855708162)
XLA Ops:
  0.0 89.1 %shard_map.118 = bf16[4,32,2048]{2,1,0:T(8,128)(2,1)} custom-call(bf16[4,32,2048]{2,1,0:T(8,128)(2,1)} %tok_ref.1, f32[1,2048]{1,0:T(1,128)} %bitcast.5, bf16[2048,256]{1,0:T(8,128)(2,1)} %ew_hbm.1, bf16[2048,256]{1,0:T(8,128)(2,1)} %vw_hbm.1, f32[4,256]{1,0:T(4,128)} %taps_ref.1, f32[1,256]{1,0:T(1,128)} %bitcast.6, bf16[2,128,128]{2,1,0:T(8,128)(2,1)} %rw_ref.1, ...), custom_call_target="tpu_custom_call" | custom-call | tf_op jit(solution)/shard_map/pallas_call | solution.py:367
  89.1 1.9 %copy.14 = bf16[4,32,2048]{2,1,0:T(8,128)(2,1)} copy(bf16[4,32,2048]{2,1,0:T(8,128)(2,1)} %shard_map.118) | data formatting | bytes 1048576
